TPU v7x, 32 devices: a whole 2x2x4 slice. The times are simulated.
32 devices in a mesh: sp: 4 (over z), dp: 8 (over y, x, core).
Axes of the slice: x: 2, y: 2, z: 4, core: 2. Of those that a mesh axis runs over, the one named last changes fastest.
Arguments:
- mixing_input: bfloat16 [8, 512, 2048], P('dp', 'sp'), may hold values from -6 to 6
- cotangent: bfloat16 [8, 512, 2048], P('dp', 'sp'), may hold values from -6 to 6
- filter_taps: bfloat16 [4, 2048], P(None, 'sp'), may hold values from -3 to 3
- recurrence_gate_map: bfloat16 [2, 16, 128, 128], P(None, 'sp'), may hold values from -0.5 to 0.5
- input_gate_map: bfloat16 [2, 16, 128, 128], P(None, 'sp'), may hold values from -0.5 to 0.5
- decay_logit_param: float32 [2, 2048], P(None, 'sp')
- spike_decay: float32 [8, 16, 512], P('dp', 'sp'), may hold values from -2 to -0.0001953125
Outputs:
- grad_input: bfloat16 [8, 512, 2048], P('dp', 'sp')
- grad_rate_map: float32 [2, 16, 128, 128], P(None, 'sp')
- grad_input_map: float32 [2, 16, 128, 128], P(None, 'sp')
- grad_conv_taps: float32 [4, 2048], P(None, 'sp')
All inputs are finite; a program needn't handle non-finite values.
Results may differ from a plain program's by a relative error of at most 0.0075.
Values may be sent and summed in bfloat16 or wider, within the bound.
A program may use at most 64 MiB of HBM per device.

v0:
```python
import functools
import math

import jax
import jax.numpy as jnp
from jax import lax
from jax.experimental import pallas as pl
from jax.experimental.pallas import tpu as pltpu
from jax.sharding import PartitionSpec as P

SEG = 8
LANES = 128
UNROLL = 4


def shift_segments(rows, down):
    index = lax.broadcasted_iota(jnp.int32, rows.shape, 0)
    if down:
        return jnp.where(index == 0, 0.0, pltpu.roll(rows, 1, 0))
    return jnp.where(index == SEG - 1, 0.0, pltpu.roll(rows, SEG - 1, 0))


def carry_in(product, total, down):
    p = shift_segments(product, down)
    q = shift_segments(total, down)
    for step in (1, 2, 4):
        amount = step if down else SEG - step
        q = q + p * pltpu.roll(q, amount, 0)
        p = p * pltpu.roll(p, amount, 0)
    return q


def load_head(x_ref, c_ref, s, rows):
    pitch = rows + SEG
    for seg in range(SEG):
        s["xs"][pl.ds(seg * pitch, rows), :] = x_ref[pl.ds(seg * rows, rows), :].astype(jnp.float32)
        s["cs"][pl.ds(seg * pitch, rows), :] = c_ref[pl.ds(seg * rows, rows), :].astype(jnp.float32)


def head_compute(s, rows, spike_ref, taps, keep, weights, out_gi):
    f32, bf16 = jnp.float32, jnp.bfloat16
    pitch = rows + SEG
    length = rows * SEG
    tile = (SEG, LANES)
    tap = [jnp.broadcast_to(taps[k : k + 1, :], tile) for k in range(4)]
    logit = keep
    log_keep = jnp.minimum(logit, 0.0) - jnp.log1p(jnp.exp(-jnp.abs(logit)))
    k4 = [jnp.broadcast_to(4.0 * log_keep[d : d + 1, :], tile) for d in range(2)]
    k2 = [jnp.broadcast_to(2.0 * log_keep[d : d + 1, :], tile) for d in range(2)]

    for j in range(4):
        s["wc"][:, j * LANES : (j + 1) * LANES] = weights[j]()
    for b in range(length // LANES):
        s["spk"][pl.ds(b * (LANES // SEG), LANES // SEG)] = jnp.transpose(
            jnp.broadcast_to(spike_ref[b : b + 1, :], (LANES, LANES))
        ).reshape(LANES // SEG, SEG, LANES)

    def permute(i, _):
        for u in range(UNROLL):
            r = i * UNROLL + u
            s["xp"][r + 2] = s["xs"][pl.ds(r, SEG, stride=pitch), :]
            s["cp"][r] = s["cs"][pl.ds(r, SEG, stride=pitch), :]
        return 0

    lax.fori_loop(0, rows // UNROLL, permute, 0)
    xp = s["xp"]
    xp[0] = shift_segments(xp[rows], True)
    xp[1] = shift_segments(xp[rows + 1], True)
    xp[rows + 2] = shift_segments(xp[2], False)

    def conv(i, _):
        for u in range(0, UNROLL, 2):
            r = i * UNROLL + u
            pair = []
            for w in range(2):
                acc = xp[r + w] * tap[0]
                for k in range(1, 4):
                    acc = acc + xp[r + w + k] * tap[k]
                pair.append(acc)
            start = pl.multiple_of(r * SEG, 2 * SEG)
            s["vb"][pl.ds(start, 2 * SEG), :] = jnp.concatenate(pair, axis=0).astype(bf16)
        return 0

    lax.fori_loop(0, rows // UNROLL, conv, 0)

    chunk = 256

    def gates(i, _):
        start = pl.multiple_of(i * chunk, chunk)
        s["pre"][pl.ds(start, chunk), :] = jnp.dot(
            s["vb"][pl.ds(start, chunk), :], s["wc"][...], preferred_element_type=f32
        )
        return 0

    lax.fori_loop(0, length // chunk, gates, 0)

    def first(i, carry):
        p0, s0, w0, p1, s1, w1 = carry
        for u in range(0, UNROLL, 2):
            base = i * UNROLL + u
            start = pl.multiple_of(base * SEG, 2 * SEG)
            v_pair = s["vb"][pl.ds(start, 2 * SEG), :].astype(f32)
            for w in range(2):
                r = base + w
                row = pl.multiple_of(r * SEG, SEG)
                v = v_pair[w * SEG : (w + 1) * SEG]
                c = s["cp"][r]
                spike = s["spk"][r]
                found = []
                for d in range(2):
                    th = jnp.tanh(0.5 * s["pre"][pl.ds(row, SEG), 2 * d * LANES : (2 * d + 1) * LANES])
                    tg = jnp.tanh(0.5 * s["pre"][pl.ds(row, SEG), (2 * d + 1) * LANES : (2 * d + 2) * LANES])
                    log_decay = k4[d] * th + (k4[d] + spike)
                    decay = jnp.exp(log_decay)
                    decay2 = decay * decay
                    m2 = -jnp.tanh(log_decay) * (1.0 + decay2)
                    inverse = lax.rsqrt(m2)
                    half = 0.5 * tg
                    gate = 0.5 + half
                    slope = (m2 * inverse) * gate
                    source = slope * v
                    s["dec"][d, r] = decay
                    s["src"][d, r] = source
                    s["slope"][d, r] = slope
                    s["second"][d, r] = gate * v * decay2 * inverse
                    s["rate"][d, r] = k2[d] * (1.0 - th * th)
                    s["gate"][d, r] = source * (0.5 - half)
                    found.append((decay, source))
                (d0, g0), (d1, g1) = found
                s0 = d0 * s0 + g0
                p0 = p0 * d0
                w0 = w0 + p0 * c
                w1 = d1 * (c + w1)
                s1 = s1 + p1 * g1
                p1 = p1 * d1
        return p0, s0, w0, p1, s1, w1

    zero = jnp.zeros(tile, f32)
    one = jnp.ones(tile, f32)
    p0, s0, w0, p1, s1, w1 = lax.fori_loop(0, rows // UNROLL, first, (one, zero, zero, one, zero, zero))
    s0 = carry_in(p0, s0, True)
    w0 = carry_in(p0, w0, False)
    w1 = carry_in(p1, w1, True)
    s1 = carry_in(p1, s1, False)

    def forward(i, carry):
        state, back = carry
        for u in range(UNROLL):
            r = i * UNROLL + u
            moved = s["dec"][0, r] * state
            state = moved + s["src"][0, r]
            s["rate"][0, r] = (moved - s["second"][0, r]) * s["rate"][0, r]
            adjoint = s["cp"][r] + back
            back = s["dec"][1, r] * adjoint
            s["adj"][r] = adjoint
        return state, back

    lax.fori_loop(0, rows // UNROLL, forward, (s0, w1))

    def reverse(i, carry):
        state, back = carry
        for u in range(UNROLL - 2, -2, -2):
            base = rows - (i + 1) * UNROLL + u
            parts = [None, None]
            for w in (1, 0):
                r = base + w
                adjoint = s["cp"][r] + back
                back = s["dec"][0, r] * adjoint
                moved = s["dec"][1, r] * state
                state = moved + s["src"][1, r]
                other = s["adj"][r]
                s["vg"][r + 1] = adjoint * s["slope"][0, r] + other * s["slope"][1, r]
                parts[w] = (
                    adjoint * s["rate"][0, r],
                    adjoint * s["gate"][0, r],
                    other * ((moved - s["second"][1, r]) * s["rate"][1, r]),
                    other * s["gate"][1, r],
                )
            start = pl.multiple_of(base * SEG, 2 * SEG)
            for j in range(4):
                s["back"][pl.ds(start, 2 * SEG), j * LANES : (j + 1) * LANES] = jnp.concatenate(
                    [parts[0][j], parts[1][j]], axis=0
                ).astype(bf16)
        return state, back

    lax.fori_loop(0, rows // UNROLL, reverse, (s1, w0))

    vg = s["vg"]

    def through(i, _):
        start = pl.multiple_of(i * chunk, chunk)
        part = lax.dot_general(
            s["back"][pl.ds(start, chunk), :],
            s["wc"][...],
            (((1,), (1,)), ((), ())),
            preferred_element_type=f32,
        )
        where = pl.ds(i * (chunk // SEG) + 1, chunk // SEG)
        vg[where] = vg[where] + part.reshape(chunk // SEG, SEG, LANES)
        return 0

    lax.fori_loop(0, length // chunk, through, 0)
    vg[0] = shift_segments(vg[rows], True)
    vg[rows + 1] = shift_segments(vg[1], False)
    vg[rows + 2] = shift_segments(vg[2], False)

    maps = lax.dot_general(
        s["vb"][...], s["back"][...], (((0,), (0,)), ((), ())), preferred_element_type=f32
    )

    def last(i, sums):
        sums = list(sums)
        for u in range(UNROLL):
            r = i * UNROLL + u
            here = vg[r + 1]
            acc = vg[r + 3] * tap[0] + vg[r + 2] * tap[1] + here * tap[2] + vg[r] * tap[3]
            s["xs"][pl.ds(r, SEG, stride=pitch), :] = acc
            for k in range(4):
                sums[k] = sums[k] + xp[r + k] * here
        return tuple(sums)

    sums = lax.fori_loop(0, rows // UNROLL, last, (zero,) * 4)
    for seg in range(SEG):
        out_gi(seg, s["xs"][pl.ds(seg * pitch, rows), :].astype(bf16))
    tap_rows = jnp.concatenate([jnp.sum(a, axis=0, keepdims=True) for a in sums], axis=0)
    return maps, tap_rows


def head_scratch(rows):
    f32, bf16 = jnp.float32, jnp.bfloat16
    length = rows * SEG
    pitch = rows + SEG
    per = lambda n: pltpu.VMEM((n, SEG, LANES), f32)
    both = lambda: pltpu.VMEM((2, rows, SEG, LANES), f32)
    return dict(
        xs=pltpu.VMEM((SEG * pitch, LANES), f32),
        cs=pltpu.VMEM((SEG * pitch, LANES), f32),
        xp=per(rows + 3),
        cp=per(rows),
        spk=per(rows),
        vb=pltpu.VMEM((length, LANES), bf16),
        wc=pltpu.VMEM((LANES, 4 * LANES), bf16),
        pre=pltpu.VMEM((length, 4 * LANES), f32),
        dec=both(),
        src=both(),
        slope=both(),
        second=both(),
        rate=both(),
        gate=both(),
        adj=per(rows),
        vg=per(rows + 3),
        back=pltpu.VMEM((length, 4 * LANES), bf16),
    )


def head_kernel(rows, norm, x_ref, c_ref, taps_ref, rmap_ref, imap_ref, keep_ref, spike_ref,
                gi_ref, grate_ref, ginput_ref, gtaps_ref, s):
    load_head(x_ref, c_ref, s, rows)

    def out_gi(seg, value):
        gi_ref[pl.ds(seg * rows, rows), :] = value

    weights = [
        lambda: rmap_ref[0, 0], lambda: imap_ref[0, 0],
        lambda: rmap_ref[1, 0], lambda: imap_ref[1, 0],
    ]
    maps, tap_rows = head_compute(
        s, rows, spike_ref.at[0], taps_ref[...], keep_ref[...], weights, out_gi
    )
    maps = maps * norm
    for d in range(2):
        grate_ref[d, 0] = maps[:, 2 * d * LANES : (2 * d + 1) * LANES]
        ginput_ref[d, 0] = maps[:, (2 * d + 1) * LANES : (2 * d + 2) * LANES]
    gtaps_ref[...] = tap_rows * norm


def body(mixing_input, cotangent, filter_taps, recurrence_gate_map, input_gate_map,
         decay_logit_param, spike_decay):
    heads = recurrence_gate_map.shape[1]
    seq_x = lax.all_to_all(mixing_input, "sp", split_axis=2, concat_axis=1, tiled=True)[0]
    seq_c = lax.all_to_all(cotangent, "sp", split_axis=2, concat_axis=1, tiled=True)[0]
    length, width = seq_x.shape
    rows = length // SEG
    norm = 1.0 / math.sqrt(lax.axis_size("dp") * length)
    taps = filter_taps.astype(jnp.float32)
    spike = jnp.swapaxes(spike_decay[0].reshape(heads, SEG, rows), 1, 2)
    spike = spike.reshape(heads, length // LANES, LANES)
    f32 = jnp.float32
    gi, grate, ginput, gtaps = pl.pallas_call(
        functools.partial(head_kernel, rows, norm),
        grid=(heads,),
        in_specs=[
            pl.BlockSpec((length, LANES), lambda h: (0, h)),
            pl.BlockSpec((length, LANES), lambda h: (0, h)),
            pl.BlockSpec((4, LANES), lambda h: (0, h)),
            pl.BlockSpec((2, 1, LANES, LANES), lambda h: (0, h, 0, 0)),
            pl.BlockSpec((2, 1, LANES, LANES), lambda h: (0, h, 0, 0)),
            pl.BlockSpec((2, LANES), lambda h: (0, h)),
            pl.BlockSpec((1, length // LANES, LANES), lambda h: (h, 0, 0)),
        ],
        out_specs=[
            pl.BlockSpec((length, LANES), lambda h: (0, h)),
            pl.BlockSpec((2, 1, LANES, LANES), lambda h: (0, h, 0, 0)),
            pl.BlockSpec((2, 1, LANES, LANES), lambda h: (0, h, 0, 0)),
            pl.BlockSpec((4, LANES), lambda h: (0, h)),
        ],
        out_shape=[
            jax.ShapeDtypeStruct((length, width), jnp.bfloat16),
            jax.ShapeDtypeStruct((2, heads, LANES, LANES), f32),
            jax.ShapeDtypeStruct((2, heads, LANES, LANES), f32),
            jax.ShapeDtypeStruct((4, width), f32),
        ],
        scratch_shapes=[head_scratch(rows)],
        compiler_params=pltpu.CompilerParams(
            dimension_semantics=("arbitrary",), vmem_limit_bytes=50 * 1024 * 1024
        ),
        name="heads",
    )(seq_x, seq_c, taps, recurrence_gate_map, input_gate_map, decay_logit_param, spike)
    grate, ginput, gtaps = lax.psum((grate, ginput, gtaps), "dp")
    grad_input = lax.all_to_all(gi[None], "sp", split_axis=1, concat_axis=2, tiled=True)
    return grad_input, grate, ginput, gtaps


def solution(mesh):
    return jax.shard_map(
        body,
        mesh=mesh,
        in_specs=(
            P("dp", "sp", None),
            P("dp", "sp", None),
            P(None, "sp"),
            P(None, "sp", None, None),
            P(None, "sp", None, None),
            P(None, "sp"),
            P("dp", "sp", None),
        ),
        out_specs=(
            P("dp", "sp", None),
            P(None, "sp", None, None),
            P(None, "sp", None, None),
            P(None, "sp"),
        ),
        check_vma=False,
    )
```

profile of v0, /device:TPU:0, one launch (start us, length us, event | category | flops | bytes accessed | tf_op | source)
XLA Modules:
  0.0 159.5 jit_solution(16184358141930898502)
XLA Ops:
  7.2 2.4 %copy.32 = bf16[1,128,2048]{1,0,2:T(2,128)(2,1)S(1)} copy(bf16[1,128,2048]{2,1,0:T(8,128)(2,1)} %param.7) | data formatting | bytes 1048576 | tf_op args[0]
  9.5 0.5 broadcast
  10.0 11.5 %reduce = bf16[2048,128]{1,0:T(8,128)(2,1)S(1)} reduce(bf16[2048,1,128]{2,1,0:T(2,128)(2,1)S(1)} %bitcast.28, bf16[]{:T(256)} %broadcast), dimensions={1}, to_apply=%bitcast.14.reduce_sub_computation | reduce | bytes 1048578
  21.6 0.9 reshape.14
  22.5 6.5 %all-to-all-start = ((bf16[4,2,32768]{2,1,0:T(2,128)(2,1)}), bf16[4,2,32768]{2,1,0:T(2,128)(2,1)S(1)}, u32[]{:S(2)}, u32[]{:S(2)}) async-start(bf16[4,2,32768]{2,1,0:T(2,128)(2,1)} %reshape.14), calls=%async_computation | async-start | bytes 1048576 | tf_op jit(solution)/shard_map/all_to_all | solution.py:280
  29.0 0.7 copy.34
  29.7 11.5 %reduce.1 = bf16[2048,128]{1,0:T(8,128)(2,1)S(1)} reduce(bf16[2048,1,128]{2,1,0:T(2,128)(2,1)S(1)} %bitcast.30, bf16[]{:T(256)} %broadcast), dimensions={1}, to_apply=%bitcast.16.reduce_sub_computation | reduce | bytes 1048578
  41.3 0.9 reshape.16
  42.2 1.3 all-to-all-done
  43.5 3.9 %all-to-all-start.1 = ((bf16[4,2,32768]{2,1,0:T(2,128)(2,1)}), bf16[4,2,32768]{2,1,0:T(2,128)(2,1)S(1)}, u32[]{:S(2)}, u32[]{:S(2)}) async-start(bf16[4,2,32768]{2,1,0:T(2,128)(2,1)} %reshape.16), calls=%async_computation.1 | async-start | bytes 1048576 | tf_op jit(solution)/shard_map/all_to_all | solution.py:281
  47.4 0.7 copy-done.5
  48.3 0.1 reshape.13.spike_ref
  48.4 0.5 reshape.15
  49.0 0.2 copy.33
  49.2 12.1 %all-to-all-done.1 = bf16[4,2,32768]{2,1,0:T(2,128)(2,1)S(1)} async-done(((bf16[4,2,32768]{2,1,0:T(2,128)(2,1)}), bf16[4,2,32768]{2,1,0:T(2,128)(2,1)S(1)}, u32[]{:S(2)}, u32[]{:S(2)}) %all-to-all-start.1) | async-done | bytes 524320 | tf_op jit(solution)/shard_map/all_to_all | solution.py:281
  61.3 0.5 reshape.17
  62.0 0.2 copy.35
  62.2 0.7 copy-done
  63.0 14.8 %heads.1 = (bf16[512,512]{1,0:T(8,128)(2,1)S(1)}, f32[2,4,128,128]{3,2,1,0:T(8,128)}, f32[2,4,128,128]{3,2,1,0:T(8,128)}, f32[4,512]{1,0:T(4,128)S(1)}) custom-call(bf16[512,512]{1,0:T(8,128)(2,1)S(1)} %bitcast.22, bf16[512,512]{1,0:T(8,128)(2,1)S(1)} %bitcast.23, f32[4,512]{1,0:T(4,128)S(1)} %convert_element_type.3.taps_ref, ...), custom_call_target="tpu_custom_call" | custom-call | tf_op jit(solution)/shard_map/heads/pallas_call | solution.py:289
  77.8 0.8 copy.44
  78.6 3.8 %reduce.2 = bf16[512,512]{1,0:T(8,128)(2,1)S(1)} reduce(bf16[512,1,512]{2,1,0:T(2,128)(2,1)S(1)} %bitcast.29, bf16[]{:T(256)} %broadcast), dimensions={1}, to_apply=%bitcast.21.reduce_sub_computation | reduce | bytes 1048578
  82.4 1.2 reshape.18
  83.6 3.5 %all-to-all-start.2 = ((bf16[4,2,32768]{2,1,0:T(2,128)(2,1)}), bf16[4,2,32768]{2,1,0:T(2,128)(2,1)S(1)}, u32[]{:S(2)}, u32[]{:S(2)}) async-start(bf16[4,2,32768]{2,1,0:T(2,128)(2,1)} %reshape.18), calls=%async_computation.2 | async-start | bytes 1048576 | tf_op jit(solution)/shard_map/all_to_all | solution.py:320
  87.1 0.7 all-reduce.3.cloned.1.call-update
  87.8 13.9 %psum.23 = f32[4,512]{1,0:T(4,128)} all-reduce(f32[4,512]{1,0:T(4,128)S(1)} %get-tuple-element.11), channel_id=1, replica_groups=mesh['sp'=4,'dp'=8] {'dp'}, use_global_device_ids=true, to_apply=%region_2.0 | all-reduce | flops 2048 | bytes 16384 | tf_op jit(solution)/shard_map/psum | solution.py:319
  101.7 0.5 reshape.19
  102.3 0.1 copy.42
  102.4 0.3 copy.38
  102.7 1.0 copy.39
  103.7 46.2 %all-reduce.3.cloned.1.call-done = (f32[2,4,128,128]{3,2,1,0:T(8,128)}, f32[2,4,128,128]{3,2,1,0:T(8,128)}) async-done(((f32[2,4,128,128]{3,2,1,0:T(8,128)}, f32[2,4,128,128]{3,2,1,0:T(8,128)}), (f32[2,4,128,128]{3,2,1,0:T(8,128)}, f32[2,4,128,128]{3,2,1,0:T(8,128)})) %all-reduce.3.cloned.1.call-update) | async-done | bytes 1048592 | tf_op jit(solution)/shard_map/psum | solution.py:319
  149.9 1.9 %copy.47 = f32[2,4,128,128]{3,2,1,0:T(8,128)} copy(f32[2,4,128,128]{3,2,1,0:T(8,128)} %get-tuple-element.19) | data formatting | bytes 1048576
  151.8 0.8 copy.48
  (19 shorter events, 0.5 us)
Async XLA Ops:
  22.5 6.5 %copy-start.3 = (bf16[1,128,2048]{2,1,0:T(8,128)(2,1)S(1)}, bf16[1,128,2048]{2,1,0:T(8,128)(2,1)}, u32[]{:S(2)}) copy-start(bf16[1,128,2048]{2,1,0:T(8,128)(2,1)} %param.8) | copy-start | bytes 1572868
  22.5 21.0 %all-to-all-start = ((bf16[4,2,32768]{2,1,0:T(2,128)(2,1)}), bf16[4,2,32768]{2,1,0:T(2,128)(2,1)S(1)}, u32[]{:S(2)}, u32[]{:S(2)}) async-start(bf16[4,2,32768]{2,1,0:T(2,128)(2,1)} %reshape.14), calls=%async_computation | async-start | bytes 1048576 | tf_op jit(solution)/shard_map/all_to_all | solution.py:280
  42.2 5.2 %copy-start.6 = (bf16[4,512]{1,0:T(4,128)(2,1)S(1)}, bf16[4,512]{1,0:T(4,128)(2,1)}, u32[]{:S(2)}) copy-start(bf16[4,512]{1,0:T(4,128)(2,1)} %param.9) | copy-start | bytes 12292
  43.5 17.9 %all-to-all-start.1 = ((bf16[4,2,32768]{2,1,0:T(2,128)(2,1)}), bf16[4,2,32768]{2,1,0:T(2,128)(2,1)S(1)}, u32[]{:S(2)}, u32[]{:S(2)}) async-start(bf16[4,2,32768]{2,1,0:T(2,128)(2,1)} %reshape.16), calls=%async_computation.1 | async-start | bytes 1048576 | tf_op jit(solution)/shard_map/all_to_all | solution.py:281
  47.4 0.7 copy-start.5
  61.9 1.0 copy-start
  62.0 1.0 copy-start.1
  62.0 1.0 copy-start.2
  83.6 18.1 %all-to-all-start.2 = ((bf16[4,2,32768]{2,1,0:T(2,128)(2,1)}), bf16[4,2,32768]{2,1,0:T(2,128)(2,1)S(1)}, u32[]{:S(2)}, u32[]{:S(2)}) async-start(bf16[4,2,32768]{2,1,0:T(2,128)(2,1)} %reshape.18), calls=%async_computation.2 | async-start | bytes 1048576 | tf_op jit(solution)/shard_map/all_to_all | solution.py:320
  87.1 62.8 %all-reduce.3.cloned.1.call-start = ((), (), s32[]{:S(2)}) async-start(), calls=%async_computation.3 | async-start | bytes 2097152 | tf_op jit(solution)/shard_map/psum | solution.py:319
  149.9 1.9 %copy-start.4 = (f32[2,4,128,128]{3,2,1,0:T(8,128)S(1)}, f32[2,4,128,128]{3,2,1,0:T(8,128)}, u32[]{:S(2)}) copy-start(f32[2,4,128,128]{3,2,1,0:T(8,128)} %get-tuple-element.20) | copy-start | bytes 1572868
Sparse Core Ops, SparseCore 0:
  91.7 58.1 all-reduce.2
where the time goes:
time: 160 us; the launch traced here: 159 us
  waiting for transfers between devices  60.3 us (38%)
  other arithmetic  26.9 us (17%)
  local copies, waits for them, and re-layouts  15.5 us (10%)
  Pallas kernels  14.8 us (9%)
  between operations  14.2 us (9%)
  starting transfers between devices  13.9 us (9%)
  blocking collectives  13.9 us (9%)
    psum x1, waiting for transfers between devices, body(): grate, ginput, gtaps = lax.psum((grate, ginput, gtaps), 'dp')  46.2 us
    unnamed x3, other arithmetic  26.9 us
    pallas_call x1, Pallas kernels, body(): pl.pallas_call(functools.partial(head_kernel, rows, norm), grid=(heads,),...  14.8 us
    psum x1, blocking collectives, body(): grate, ginput, gtaps = lax.psum((grate, ginput, gtaps), 'dp')  13.9 us
    unnamed x29, local copies, waits for them, and re-layouts  13.7 us
    all_to_all x1, waiting for transfers between devices, body(): lax.all_to_all(cotangent, 'sp', split_axis=2, concat_axis=1, tiled=True)[0]  12.1 us
    all_to_all x1, starting transfers between devices, body(): lax.all_to_all(mixing_input, 'sp', split_axis=2, concat_axis=1, tiled=True)  6.48 us
    all_to_all x1, starting transfers between devices, body(): lax.all_to_all(cotangent, 'sp', split_axis=2, concat_axis=1, tiled=True)[0]  3.95 us
  transfers between devices with their start and end apart: 4, of which 3 were waited for; matrix products, arithmetic and copies ran while one was open for 10% of the time, Pallas kernels for 0%

commit v1 on v0

--- a/solution.py
+++ b/solution.py
@@ -37,7 +37,7 @@
         s["cs"][pl.ds(seg * pitch, rows), :] = c_ref[pl.ds(seg * rows, rows), :].astype(jnp.float32)
 
 
-def head_compute(s, rows, spike_ref, taps, keep, weights, out_gi):
+def head_compute(s, rows, spike_row, taps, keep, weights, out_gi):
     f32, bf16 = jnp.float32, jnp.bfloat16
     pitch = rows + SEG
     length = rows * SEG
@@ -50,16 +50,22 @@
 
     for j in range(4):
         s["wc"][:, j * LANES : (j + 1) * LANES] = weights[j]()
+    piece = min(rows, LANES)
     for b in range(length // LANES):
-        s["spk"][pl.ds(b * (LANES // SEG), LANES // SEG)] = jnp.transpose(
-            jnp.broadcast_to(spike_ref[b : b + 1, :], (LANES, LANES))
-        ).reshape(LANES // SEG, SEG, LANES)
+        block = jnp.transpose(
+            jnp.broadcast_to(spike_row(b), (LANES, LANES))
+        )
+        for e in range(LANES // piece):
+            at = b * LANES + e * piece
+            where = at // rows * pitch + at % rows
+            s["ss"][pl.ds(where, piece), :] = block[e * piece : (e + 1) * piece]
 
     def permute(i, _):
         for u in range(UNROLL):
             r = i * UNROLL + u
             s["xp"][r + 2] = s["xs"][pl.ds(r, SEG, stride=pitch), :]
             s["cp"][r] = s["cs"][pl.ds(r, SEG, stride=pitch), :]
+            s["spk"][r] = s["ss"][pl.ds(r, SEG, stride=pitch), :]
         return 0
 
     lax.fori_loop(0, rows // UNROLL, permute, 0)
@@ -235,6 +241,7 @@
     return dict(
         xs=pltpu.VMEM((SEG * pitch, LANES), f32),
         cs=pltpu.VMEM((SEG * pitch, LANES), f32),
+        ss=pltpu.VMEM((SEG * pitch, LANES), f32),
         xp=per(rows + 3),
         cp=per(rows),
         spk=per(rows),
@@ -253,72 +260,232 @@
     )
 
 
-def head_kernel(rows, norm, x_ref, c_ref, taps_ref, rmap_ref, imap_ref, keep_ref, spike_ref,
-                gi_ref, grate_ref, ginput_ref, gtaps_ref, s):
-    load_head(x_ref, c_ref, s, rows)
-
-    def out_gi(seg, value):
-        gi_ref[pl.ds(seg * rows, rows), :] = value
-
-    weights = [
-        lambda: rmap_ref[0, 0], lambda: imap_ref[0, 0],
-        lambda: rmap_ref[1, 0], lambda: imap_ref[1, 0],
-    ]
-    maps, tap_rows = head_compute(
-        s, rows, spike_ref.at[0], taps_ref[...], keep_ref[...], weights, out_gi
-    )
-    maps = maps * norm
-    for d in range(2):
-        grate_ref[d, 0] = maps[:, 2 * d * LANES : (2 * d + 1) * LANES]
-        ginput_ref[d, 0] = maps[:, (2 * d + 1) * LANES : (2 * d + 2) * LANES]
-    gtaps_ref[...] = tap_rows * norm
+def whole_kernel(sizes, norm, x_ref, c_ref, taps_ref, rmap_ref, imap_ref, keep_ref, spike_ref,
+                 out_ref, grate_ref, ginput_ref, gtaps_ref, s):
+    n, m, heads, tok, rows, q = sizes
+    f32, bf16 = jnp.float32, jnp.bfloat16
+    me = lax.axis_index("sp")
+    mine = lax.axis_index("dp")
+    cols = heads * LANES
+    inputs = (x_ref, c_ref)
+    wire = s["wbuf"].dtype
+
+    barrier = pltpu.get_barrier_semaphore()
+
+    def greet_sp(o, _):
+        pl.semaphore_signal(barrier, inc=1, device_id={"sp": lax.rem(me + o, n)},
+                            device_id_type=pl.DeviceIdType.MESH)
+        return 0
+
+    def greet_dp(o, _):
+        pl.semaphore_signal(barrier, inc=1, device_id={"dp": lax.rem(mine + o, m)},
+                            device_id_type=pl.DeviceIdType.MESH)
+        return 0
+
+    lax.fori_loop(1, n, greet_sp, 0)
+    lax.fori_loop(1, m, greet_dp, 0)
+    pl.semaphore_wait(barrier, n + m - 2)
+
+    def lanes_of(device, h):
+        return pl.ds(pl.multiple_of(device * cols + h * LANES, LANES), LANES)
+
+    def tokens_of(device):
+        return pl.ds(pl.multiple_of(device * tok, tok), tok)
+
+    def part_of(device):
+        return pl.ds(pl.multiple_of(device * q, q), q)
+
+    def in_copy(a, h, o):
+        peer = lax.rem(me + o, n)
+        return pltpu.make_async_remote_copy(
+            src_ref=inputs[a].at[0, :, lanes_of(peer, h)],
+            dst_ref=s["xin"].at[a, h, tokens_of(me), :],
+            send_sem=s["in_send"].at[a, h, o - 1],
+            recv_sem=s["in_recv"].at[a, h, o - 1],
+            device_id={"sp": peer},
+            device_id_type=pl.DeviceIdType.MESH,
+        )
+
+    def out_copy(h, o):
+        peer = lax.rem(me + o, n)
+        return pltpu.make_async_remote_copy(
+            src_ref=s["gout"].at[h, tokens_of(peer), :],
+            dst_ref=out_ref.at[0, :, lanes_of(me, h)],
+            send_sem=s["out_send"].at[h, o - 1],
+            recv_sem=s["out_recv"].at[h, o - 1],
+            device_id={"sp": peer},
+            device_id_type=pl.DeviceIdType.MESH,
+        )
+
+    def rs_copy(h, o):
+        peer = lax.rem(mine + o, m)
+        return pltpu.make_async_remote_copy(
+            src_ref=s["wbuf"].at[h, part_of(peer), :],
+            dst_ref=s["rbuf"].at[h, o - 1],
+            send_sem=s["rs_send"].at[h, o - 1],
+            recv_sem=s["rs_recv"].at[h, o - 1],
+            device_id={"dp": peer},
+            device_id_type=pl.DeviceIdType.MESH,
+        )
+
+    def ag_copy(h, o):
+        peer = lax.rem(mine + o, m)
+        return pltpu.make_async_remote_copy(
+            src_ref=s["gbuf"].at[h, part_of(mine), :],
+            dst_ref=s["gbuf"].at[h, part_of(mine), :],
+            send_sem=s["ag_send"].at[h, o - 1],
+            recv_sem=s["ag_recv"].at[h, o - 1],
+            device_id={"dp": peer},
+            device_id_type=pl.DeviceIdType.MESH,
+        )
+
+    def tap_copy(o):
+        peer = lax.rem(mine + o, m)
+        return pltpu.make_async_remote_copy(
+            src_ref=s["tbuf"].at[mine],
+            dst_ref=s["tbuf"].at[mine],
+            send_sem=s["tap_send"].at[o - 1],
+            recv_sem=s["tap_recv"].at[o - 1],
+            device_id={"dp": peer},
+            device_id_type=pl.DeviceIdType.MESH,
+        )
+
+    def each(count, act):
+        def step(o, _):
+            act(o)
+            return 0
+
+        lax.fori_loop(1, count, step, 0)
+
+    for h in range(heads):
+        for a in range(2):
+            each(n, lambda o: in_copy(a, h, o).start())
+    for h in range(heads):
+        for a in range(2):
+            s["xin"][a, h, tokens_of(me), :] = inputs[a][0, :, lanes_of(me, h)]
+
+    def finish_rs(h):
+        each(m, lambda o: rs_copy(h, o).wait_recv())
+
+        def add(o, total):
+            return total + s["rbuf"][h, o - 1].astype(f32)
+
+        total = lax.fori_loop(1, m, add, s["wbuf"][h, part_of(mine), :].astype(f32))
+        s["gbuf"][h, part_of(mine), :] = (total * norm).astype(wire)
+        each(m, lambda o: ag_copy(h, o).start())
+
+    def one_head(h, _):
+        for a in range(2):
+            each(n, lambda o: in_copy(a, h, o).wait_recv())
+        load_head(s["xin"].at[0, h], s["xin"].at[1, h], s, rows)
+        here = pl.ds(pl.multiple_of(h * LANES, LANES), LANES)
+
+        def out_gi(seg, value):
+            s["gout"][h, pl.ds(seg * rows, rows), :] = value
+
+        weights = [
+            lambda: rmap_ref[0, h], lambda: imap_ref[0, h],
+            lambda: rmap_ref[1, h], lambda: imap_ref[1, h],
+        ]
+        maps, tap_rows = head_compute(
+            s, rows,
+            lambda b: s["spike"][h, b : b + 1, :],
+            taps_ref[:, here].astype(f32), keep_ref[:, here], weights, out_gi,
+        )
+        for j in range(4):
+            s["wbuf"][h, j * LANES : (j + 1) * LANES, :] = maps[:, j * LANES : (j + 1) * LANES].astype(wire)
+        s["tbuf"][mine, h, 0:4, :] = tap_rows * norm
+        each(n, lambda o: out_copy(h, o).start())
+        each(m, lambda o: rs_copy(h, o).start())
+        out_ref[0, :, lanes_of(me, h)] = s["gout"][h, tokens_of(me), :]
+
+        @pl.when(h > 0)
+        def _():
+            finish_rs(h - 1)
+
+        return 0
+
+    s["tbuf"][mine] = jnp.zeros(s["tbuf"].shape[1:], f32)
+    for h in range(heads):
+        for b in range(rows * SEG // LANES):
+            s["spike"][h, b : b + 1, :] = spike_ref[0, h : h + 1, b * LANES : (b + 1) * LANES]
+    lax.fori_loop(0, heads, one_head, 0)
+    each(m, lambda o: tap_copy(o).start())
+    finish_rs(heads - 1)
+    each(m, lambda o: tap_copy(o).wait_recv())
+
+    def add_taps(i, total):
+        return total + s["tbuf"][i]
+
+    sums = lax.fori_loop(1, m, add_taps, s["tbuf"][0])
+    for h in range(heads):
+        gtaps_ref[:, h * LANES : (h + 1) * LANES] = sums[h, 0:4, :]
+    for h in range(heads):
+        each(m, lambda o: ag_copy(h, o).wait_recv())
+        for d in range(2):
+            grate_ref[d, h] = s["gbuf"][h, 2 * d * LANES : (2 * d + 1) * LANES, :].astype(f32)
+            ginput_ref[d, h] = s["gbuf"][h, (2 * d + 1) * LANES : (2 * d + 2) * LANES, :].astype(f32)
+    for h in range(heads):
+        each(n, lambda o: out_copy(h, o).wait_recv())
+    for h in range(heads):
+        for a in range(2):
+            each(n, lambda o: in_copy(a, h, o).wait_send())
+        each(n, lambda o: out_copy(h, o).wait_send())
+        each(m, lambda o: rs_copy(h, o).wait_send())
+        each(m, lambda o: ag_copy(h, o).wait_send())
+    each(m, lambda o: tap_copy(o).wait_send())
 
 
 def body(mixing_input, cotangent, filter_taps, recurrence_gate_map, input_gate_map,
          decay_logit_param, spike_decay):
+    f32, bf16 = jnp.float32, jnp.bfloat16
+    n, m = lax.axis_size("sp"), lax.axis_size("dp")
     heads = recurrence_gate_map.shape[1]
-    seq_x = lax.all_to_all(mixing_input, "sp", split_axis=2, concat_axis=1, tiled=True)[0]
-    seq_c = lax.all_to_all(cotangent, "sp", split_axis=2, concat_axis=1, tiled=True)[0]
-    length, width = seq_x.shape
+    tok, width = mixing_input.shape[1:]
+    length = tok * n
     rows = length // SEG
-    norm = 1.0 / math.sqrt(lax.axis_size("dp") * length)
-    taps = filter_taps.astype(jnp.float32)
-    spike = jnp.swapaxes(spike_decay[0].reshape(heads, SEG, rows), 1, 2)
-    spike = spike.reshape(heads, length // LANES, LANES)
-    f32 = jnp.float32
-    gi, grate, ginput, gtaps = pl.pallas_call(
-        functools.partial(head_kernel, rows, norm),
-        grid=(heads,),
-        in_specs=[
-            pl.BlockSpec((length, LANES), lambda h: (0, h)),
-            pl.BlockSpec((length, LANES), lambda h: (0, h)),
-            pl.BlockSpec((4, LANES), lambda h: (0, h)),
-            pl.BlockSpec((2, 1, LANES, LANES), lambda h: (0, h, 0, 0)),
-            pl.BlockSpec((2, 1, LANES, LANES), lambda h: (0, h, 0, 0)),
-            pl.BlockSpec((2, LANES), lambda h: (0, h)),
-            pl.BlockSpec((1, length // LANES, LANES), lambda h: (h, 0, 0)),
+    q = 4 * LANES // m
+    wire = bf16 if q % 16 == 0 else f32
+    norm = 1.0 / math.sqrt(m * length)
+    dma = lambda *shape: pltpu.SemaphoreType.DMA(shape)
+    scratch = dict(
+        head_scratch(rows),
+        xin=pltpu.VMEM((2, heads, length, LANES), bf16),
+        gout=pltpu.VMEM((heads, length, LANES), bf16),
+        wbuf=pltpu.VMEM((heads, 4 * LANES, LANES), wire),
+        rbuf=pltpu.VMEM((heads, m - 1, q, LANES), wire),
+        gbuf=pltpu.VMEM((heads, 4 * LANES, LANES), wire),
+        spike=pltpu.VMEM((heads, length // LANES, LANES), f32),
+        tbuf=pltpu.VMEM((m, heads, SEG, LANES), f32),
+        in_send=dma(2, heads, n - 1),
+        in_recv=dma(2, heads, n - 1),
+        out_send=dma(heads, n - 1),
+        out_recv=dma(heads, n - 1),
+        rs_send=dma(heads, m - 1),
+        rs_recv=dma(heads, m - 1),
+        ag_send=dma(heads, m - 1),
+        ag_recv=dma(heads, m - 1),
+        tap_send=dma(m - 1),
+        tap_recv=dma(m - 1),
+    )
+    vmem = pl.BlockSpec(memory_space=pltpu.VMEM)
+    return pl.pallas_call(
+        functools.partial(whole_kernel, (n, m, heads, tok, rows, q), norm),
+        in_specs=[vmem] * 7,
+        out_specs=[vmem] * 4,
+        out_shape=[
+            jax.ShapeDtypeStruct(mixing_input.shape, bf16),
+            jax.ShapeDtypeStruct(recurrence_gate_map.shape, f32),
+            jax.ShapeDtypeStruct(recurrence_gate_map.shape, f32),
+            jax.ShapeDtypeStruct((4, heads * LANES), f32),
         ],
-        out_specs=[
-            pl.BlockSpec((length, LANES), lambda h: (0, h)),
-            pl.BlockSpec((2, 1, LANES, LANES), lambda h: (0, h, 0, 0)),
-            pl.BlockSpec((2, 1, LANES, LANES), lambda h: (0, h, 0, 0)),
-            pl.BlockSpec((4, LANES), lambda h: (0, h)),
-        ],
-        out_shape=[
-            jax.ShapeDtypeStruct((length, width), jnp.bfloat16),
-            jax.ShapeDtypeStruct((2, heads, LANES, LANES), f32),
-            jax.ShapeDtypeStruct((2, heads, LANES, LANES), f32),
-            jax.ShapeDtypeStruct((4, width), f32),
-        ],
-        scratch_shapes=[head_scratch(rows)],
+        scratch_shapes=[scratch],
         compiler_params=pltpu.CompilerParams(
-            dimension_semantics=("arbitrary",), vmem_limit_bytes=50 * 1024 * 1024
+            collective_id=0, has_side_effects=True, vmem_limit_bytes=56 * 1024 * 1024
         ),
-        name="heads",
-    )(seq_x, seq_c, taps, recurrence_gate_map, input_gate_map, decay_logit_param, spike)
-    grate, ginput, gtaps = lax.psum((grate, ginput, gtaps), "dp")
-    grad_input = lax.all_to_all(gi[None], "sp", split_axis=1, concat_axis=2, tiled=True)
-    return grad_input, grate, ginput, gtaps
+        name="heads_and_exchange",
+    )(mixing_input, cotangent, filter_taps, recurrence_gate_map, input_gate_map,
+      decay_logit_param, spike_decay)
 
 
 def solution(mesh):

time: 160 us -> 54.1 us (0.34)
  waiting for transfers between devices: 60.3 us -> 0 us
  Pallas kernels: 14.8 us -> 48.6 us
  other arithmetic: 26.9 us -> 0 us
  blocking collectives: 13.9 us -> 0 us
  starting transfers between devices: 13.9 us -> 0 us
  between operations: 14.2 us -> 0.65 us
  local copies, waits for them, and re-layouts: 15.5 us -> 4.57 us
    psum x1 -> x0, waiting for transfers between devices: 46.2 us -> none  [body(): grate, ginput, gtaps = lax.psum((grate, ginput, gtaps), 'dp')]
    pallas_call x1, Pallas kernels: 14.8 us -> 48.6 us  [body(): pl.pallas_call(functools.partial(whole_kernel, (n, m, heads, tok, rows, q...]
    unnamed x3 -> x0, other arithmetic: 26.9 us -> none
    all_to_all x3 -> x0, starting transfers between devices: 13.9 us -> none  [the longest x1 6.48 us: body(): lax.all_to_all(mixing_input, 'sp', split_axis=2, concat_axis=1, tiled=True)]
    psum x1 -> x0, blocking collectives: 13.9 us -> none  [body(): grate, ginput, gtaps = lax.psum((grate, ginput, gtaps), 'dp')]
    all_to_all x3 -> x0, waiting for transfers between devices: 13.4 us -> none  [the longest x1 12.1 us: body(): lax.all_to_all(cotangent, 'sp', split_axis=2, concat_axis=1, tiled=True)[0]]
    unnamed x29 -> x10, local copies, waits for them, and re-layouts: 13.7 us -> 4.57 us
  transfers between devices with their start and end apart: 4 -> 0, of which waited for: 3 -> 0; matrix products, arithmetic and copies ran while one was open for 10% -> 0% of each run, Pallas kernels for 0% -> 0%
where the time goes in v1:
time: 54.1 us; the launch traced here: 53.9 us
  Pallas kernels  48.6 us (90%)
  local copies, waits for them, and re-layouts  4.57 us (8%)
  between operations  0.65 us (1%)
    pallas_call x1, Pallas kernels, body(): pl.pallas_call(functools.partial(whole_kernel, (n, m, heads, tok, rows, q...  48.6 us
    unnamed x10, local copies, waits for them, and re-layouts  4.57 us

profile of v1, /device:TPU:0, one launch (start us, length us, event | category | flops | bytes accessed | tf_op | source)
XLA Modules:
  0.0 53.9 jit_solution(9348905590897441707)
XLA Ops:
  0.6 48.6 %heads_and_exchange.1 = (bf16[1,128,2048]{2,1,0:T(8,128)(2,1)}, f32[2,4,128,128]{3,2,1,0:T(8,128)}, f32[2,4,128,128]{3,2,1,0:T(8,128)}, f32[4,512]{1,0:T(4,128)}) custom-call(bf16[1,128,2048]{2,1,0:T(8,128)(2,1)} %x_ref.1, bf16[1,128,2048]{2,1,0:T(8,128)(2,1)} %c_ref.1, bf16[4,512]{1,0:T(4,128)(2,1)} %taps_ref.1, bf16[2,4,128,128]{3,2,1,0:T(8,128)(2,1)} %rmap_ref.1, ...), custom_call_target="tpu_custom_call" | custom-call | tf_op jit(solution)/shard_map/heads_and_exchange/pallas_call | solution.py:472
  49.3 0.0 copy-start.1
  49.3 1.9 %copy.15 = bf16[1,128,2048]{2,1,0:T(8,128)(2,1)} copy(bf16[1,128,2048]{2,1,0:T(8,128)(2,1)} %get-tuple-element.8) | data formatting | bytes 1048576
  51.2 0.0 copy-done.1
  51.2 0.0 copy-start
  51.2 0.8 %copy.16 = f32[2,4,128,128]{3,2,1,0:T(8,128)} copy(f32[2,4,128,128]{3,2,1,0:T(8,128)S(1)} %copy-done.1) | data formatting | bytes 1048576
  52.0 0.4 copy-done
  52.5 0.0 copy-start.2
  52.5 0.8 %copy.17 = f32[2,4,128,128]{3,2,1,0:T(8,128)} copy(f32[2,4,128,128]{3,2,1,0:T(8,128)S(1)} %copy-done) | data formatting | bytes 1048576
  53.3 0.0 copy-done.2
  53.3 0.6 %copy.18 = f32[4,512]{1,0:T(4,128)} copy(f32[4,512]{1,0:T(4,128)S(1)} %copy-done.2) | data formatting | bytes 16384
Async XLA Ops:
  49.3 2.0 %copy-start.1 = (f32[2,4,128,128]{3,2,1,0:T(8,128)S(1)}, f32[2,4,128,128]{3,2,1,0:T(8,128)}, u32[]{:S(2)}) copy-start(f32[2,4,128,128]{3,2,1,0:T(8,128)} %get-tuple-element.9) | copy-start | bytes 1572868
  51.2 1.2 %copy-start = (f32[2,4,128,128]{3,2,1,0:T(8,128)S(1)}, f32[2,4,128,128]{3,2,1,0:T(8,128)}, u32[]{:S(2)}) copy-start(f32[2,4,128,128]{3,2,1,0:T(8,128)} %get-tuple-element.10) | copy-start | bytes 1572868
  52.5 0.8 %copy-start.2 = (f32[4,512]{1,0:T(4,128)S(1)}, f32[4,512]{1,0:T(4,128)}, u32[]{:S(2)}) copy-start(f32[4,512]{1,0:T(4,128)} %get-tuple-element.11) | copy-start | bytes 24580

commit v2 on v1

--- a/solution.py
+++ b/solution.py
@@ -260,8 +260,8 @@
     )
 
 
-def whole_kernel(sizes, norm, x_ref, c_ref, taps_ref, rmap_ref, imap_ref, keep_ref, spike_ref,
-                 out_ref, grate_ref, ginput_ref, gtaps_ref, s):
+def whole_kernel(sizes, norm, x_ref, c_ref, taps_hbm, rmap_hbm, imap_hbm, keep_hbm, spike_hbm,
+                 out_ref, maps_ref, tap_ref, s):
     n, m, heads, tok, rows, q = sizes
     f32, bf16 = jnp.float32, jnp.bfloat16
     me = lax.axis_index("sp")
@@ -269,6 +269,16 @@
     cols = heads * LANES
     inputs = (x_ref, c_ref)
     wire = s["wbuf"].dtype
+
+    taps_ref, rmap_ref, imap_ref, keep_ref, spike_ref = s["small"]
+    small = [
+        pltpu.make_async_copy(source, target, s["small_sem"].at[i])
+        for i, (source, target) in enumerate(
+            zip((taps_hbm, rmap_hbm, imap_hbm, keep_hbm, spike_hbm), s["small"])
+        )
+    ]
+    for copy in small:
+        copy.start()
 
     barrier = pltpu.get_barrier_semaphore()
 
@@ -317,6 +327,19 @@
             device_id_type=pl.DeviceIdType.MESH,
         )
 
+    def own_in(a, h):
+        return pltpu.make_async_copy(
+            inputs[a].at[0, :, lanes_of(me, h)], s["xin"].at[a, h, tokens_of(me), :], s["own_in"].at[a, h]
+        )
+
+    def own_out(h):
+        return pltpu.make_async_copy(
+            s["gout"].at[h, tokens_of(me), :], out_ref.at[0, :, lanes_of(me, h)], s["own_out"].at[h]
+        )
+
+    def maps_out(h):
+        return pltpu.make_async_copy(s["gbuf"].at[h], maps_ref.at[h], s["maps_out"].at[h])
+
     def rs_copy(h, o):
         peer = lax.rem(mine + o, m)
         return pltpu.make_async_remote_copy(
@@ -362,7 +385,9 @@
             each(n, lambda o: in_copy(a, h, o).start())
     for h in range(heads):
         for a in range(2):
-            s["xin"][a, h, tokens_of(me), :] = inputs[a][0, :, lanes_of(me, h)]
+            own_in(a, h).start()
+    for copy in small:
+        copy.wait()
 
     def finish_rs(h):
         each(m, lambda o: rs_copy(h, o).wait_recv())
@@ -376,6 +401,7 @@
 
     def one_head(h, _):
         for a in range(2):
+            own_in(a, h).wait()
             each(n, lambda o: in_copy(a, h, o).wait_recv())
         load_head(s["xin"].at[0, h], s["xin"].at[1, h], s, rows)
         here = pl.ds(pl.multiple_of(h * LANES, LANES), LANES)
@@ -397,7 +423,7 @@
         s["tbuf"][mine, h, 0:4, :] = tap_rows * norm
         each(n, lambda o: out_copy(h, o).start())
         each(m, lambda o: rs_copy(h, o).start())
-        out_ref[0, :, lanes_of(me, h)] = s["gout"][h, tokens_of(me), :]
+        own_out(h).start()
 
         @pl.when(h > 0)
         def _():
@@ -417,14 +443,12 @@
     def add_taps(i, total):
         return total + s["tbuf"][i]
 
-    sums = lax.fori_loop(1, m, add_taps, s["tbuf"][0])
-    for h in range(heads):
-        gtaps_ref[:, h * LANES : (h + 1) * LANES] = sums[h, 0:4, :]
+    s["tsum"][...] = lax.fori_loop(1, m, add_taps, s["tbuf"][0])
+    tap_out = pltpu.make_async_copy(s["tsum"], tap_ref, s["small_sem"].at[0])
+    tap_out.start()
     for h in range(heads):
         each(m, lambda o: ag_copy(h, o).wait_recv())
-        for d in range(2):
-            grate_ref[d, h] = s["gbuf"][h, 2 * d * LANES : (2 * d + 1) * LANES, :].astype(f32)
-            ginput_ref[d, h] = s["gbuf"][h, (2 * d + 1) * LANES : (2 * d + 2) * LANES, :].astype(f32)
+        maps_out(h).start()
     for h in range(heads):
         each(n, lambda o: out_copy(h, o).wait_recv())
     for h in range(heads):
@@ -433,7 +457,42 @@
         each(n, lambda o: out_copy(h, o).wait_send())
         each(m, lambda o: rs_copy(h, o).wait_send())
         each(m, lambda o: ag_copy(h, o).wait_send())
+        own_out(h).wait()
+        maps_out(h).wait()
     each(m, lambda o: tap_copy(o).wait_send())
+    tap_out.wait()
+
+
+def finish_kernel(heads, in_ref, maps_ref, tap_ref, out_ref, grate_ref, ginput_ref, gtaps_ref,
+                  whole, maps, taps, grate, ginput, gtaps, sem):
+    loads = [
+        pltpu.make_async_copy(maps_ref, maps, sem.at[0]),
+        pltpu.make_async_copy(in_ref, whole, sem.at[1]),
+        pltpu.make_async_copy(tap_ref, taps, sem.at[2]),
+    ]
+    stores = [
+        pltpu.make_async_copy(grate, grate_ref, sem.at[3]),
+        pltpu.make_async_copy(ginput, ginput_ref, sem.at[4]),
+        pltpu.make_async_copy(whole, out_ref, sem.at[5]),
+        pltpu.make_async_copy(gtaps, gtaps_ref, sem.at[6]),
+    ]
+    for copy in loads:
+        copy.start()
+    loads[0].wait()
+    loads[1].wait()
+    stores[2].start()
+    for i, target in enumerate((grate, ginput)):
+        for h in range(heads):
+            for d in range(2):
+                j = 2 * d + i
+                target[d, h] = maps[h, j * LANES : (j + 1) * LANES, :].astype(jnp.float32)
+        stores[i].start()
+    loads[2].wait()
+    for h in range(heads):
+        gtaps[:, h * LANES : (h + 1) * LANES] = taps[h, 0:4, :]
+    stores[3].start()
+    for copy in stores:
+        copy.wait()
 
 
 def body(mixing_input, cotangent, filter_taps, recurrence_gate_map, input_gate_map,
@@ -457,6 +516,15 @@
         gbuf=pltpu.VMEM((heads, 4 * LANES, LANES), wire),
         spike=pltpu.VMEM((heads, length // LANES, LANES), f32),
         tbuf=pltpu.VMEM((m, heads, SEG, LANES), f32),
+        tsum=pltpu.VMEM((heads, SEG, LANES), f32),
+        small=tuple(
+            pltpu.VMEM(a.shape, a.dtype)
+            for a in (filter_taps, recurrence_gate_map, input_gate_map, decay_logit_param, spike_decay)
+        ),
+        small_sem=dma(5),
+        own_in=dma(2, heads),
+        own_out=dma(heads),
+        maps_out=dma(heads),
         in_send=dma(2, heads, n - 1),
         in_recv=dma(2, heads, n - 1),
         out_send=dma(heads, n - 1),
@@ -468,16 +536,16 @@
         tap_send=dma(m - 1),
         tap_recv=dma(m - 1),
     )
-    vmem = pl.BlockSpec(memory_space=pltpu.VMEM)
-    return pl.pallas_call(
+    anywhere = pl.BlockSpec(memory_space=pl.ANY)
+    shape = jax.ShapeDtypeStruct
+    whole, maps, sums = pl.pallas_call(
         functools.partial(whole_kernel, (n, m, heads, tok, rows, q), norm),
-        in_specs=[vmem] * 7,
-        out_specs=[vmem] * 4,
+        in_specs=[anywhere] * 7,
+        out_specs=[anywhere] * 3,
         out_shape=[
-            jax.ShapeDtypeStruct(mixing_input.shape, bf16),
-            jax.ShapeDtypeStruct(recurrence_gate_map.shape, f32),
-            jax.ShapeDtypeStruct(recurrence_gate_map.shape, f32),
-            jax.ShapeDtypeStruct((4, heads * LANES), f32),
+            shape(mixing_input.shape, bf16),
+            shape((heads, 4 * LANES, LANES), wire),
+            shape((heads, SEG, LANES), f32),
         ],
         scratch_shapes=[scratch],
         compiler_params=pltpu.CompilerParams(
@@ -486,6 +554,22 @@
         name="heads_and_exchange",
     )(mixing_input, cotangent, filter_taps, recurrence_gate_map, input_gate_map,
       decay_logit_param, spike_decay)
+    outs = [
+        shape(mixing_input.shape, bf16),
+        shape(recurrence_gate_map.shape, f32),
+        shape(recurrence_gate_map.shape, f32),
+        shape((4, heads * LANES), f32),
+    ]
+    room = lambda a: pltpu.VMEM(a.shape, a.dtype)
+    return pl.pallas_call(
+        functools.partial(finish_kernel, heads),
+        in_specs=[anywhere] * 3,
+        out_specs=[anywhere] * 4,
+        out_shape=outs,
+        scratch_shapes=[room(whole), room(maps), room(sums), room(outs[1]), room(outs[2]), room(outs[3]), dma(7)],
+        compiler_params=pltpu.CompilerParams(vmem_limit_bytes=56 * 1024 * 1024),
+        name="finish",
+    )(whole, maps, sums)
 
 
 def solution(mesh):

time: 54.1 us -> 49.8 us (0.921)
  local copies, waits for them, and re-layouts: 4.57 us -> 0 us
    unnamed x10 -> x0, local copies, waits for them, and re-layouts: 4.57 us -> none
    pallas_call x0 -> x1, Pallas kernels: none -> 2.4 us  [body(): pl.pallas_call(functools.partial(finish_kernel, heads), in_specs=[anywher...]
    pallas_call x1, Pallas kernels: 48.6 us -> 46.6 us  [body(): pl.pallas_call(functools.partial(whole_kernel, (n, m, heads, tok, rows, q...]
where the time goes in v2:
time: 49.8 us; the launch traced here: 49.6 us
  Pallas kernels  49 us (98%)
  between operations  0.64 us (1%)
    pallas_call x1, Pallas kernels, body(): pl.pallas_call(functools.partial(whole_kernel, (n, m, heads, tok, rows, q...  46.6 us
    pallas_call x1, Pallas kernels, body(): pl.pallas_call(functools.partial(finish_kernel, heads), in_specs=[anywher...  2.4 us

profile of v2, /device:TPU:0, one launch (start us, length us, event | category | flops | bytes accessed | tf_op | source)
XLA Modules:
  0.0 49.6 jit_solution(6611293597597633882)
XLA Ops:
  0.6 46.6 %heads_and_exchange.1 = (bf16[1,128,2048]{2,1,0:T(8,128)(2,1)}, bf16[4,512,128]{2,1,0:T(8,128)(2,1)}, f32[4,8,128]{2,1,0:T(8,128)}) custom-call(bf16[1,128,2048]{2,1,0:T(8,128)(2,1)} %x_ref.1, bf16[1,128,2048]{2,1,0:T(8,128)(2,1)} %c_ref.1, bf16[4,512]{1,0:T(4,128)(2,1)} %taps_hbm.1, bf16[2,4,128,128]{3,2,1,0:T(8,128)(2,1)} %rmap_hbm.1, ...), custom_call_target="tpu_custom_call" | custom-call | tf_op jit(solution)/shard_map/heads_and_exchange/pallas_call | solution.py:541
  47.2 2.4 %finish.1 = (bf16[1,128,2048]{2,1,0:T(8,128)(2,1)}, f32[2,4,128,128]{3,2,1,0:T(8,128)}, f32[2,4,128,128]{3,2,1,0:T(8,128)}, f32[4,512]{1,0:T(4,128)}) custom-call(bf16[1,128,2048]{2,1,0:T(8,128)(2,1)} %get-tuple-element.7.in_ref, bf16[4,512,128]{2,1,0:T(8,128)(2,1)} %get-tuple-element.8.maps_ref, f32[4,8,128]{2,1,0:T(8,128)} %get-tuple-element.9.tap_ref), custom_call_target="tpu_custom_call" | custom-call | tf_op jit(solution)/shard_map/finish/pallas_call | solution.py:564

commit v3 on v2

--- a/solution.py
+++ b/solution.py
@@ -277,9 +277,6 @@
             zip((taps_hbm, rmap_hbm, imap_hbm, keep_hbm, spike_hbm), s["small"])
         )
     ]
-    for copy in small:
-        copy.start()
-
     barrier = pltpu.get_barrier_semaphore()
 
     def greet_sp(o, _):
@@ -292,15 +289,25 @@
                             device_id_type=pl.DeviceIdType.MESH)
         return 0
 
+    def lanes_of(device, h):
+        return pl.ds(pl.multiple_of(device * cols + h * LANES, LANES), LANES)
+
+    def tokens_of(device):
+        return pl.ds(pl.multiple_of(device * tok, tok), tok)
+
+    def own_in(a, h):
+        return pltpu.make_async_copy(
+            inputs[a].at[0, :, lanes_of(me, h)], s["xin"].at[a, h, tokens_of(me), :], s["own_in"].at[a, h]
+        )
+
     lax.fori_loop(1, n, greet_sp, 0)
     lax.fori_loop(1, m, greet_dp, 0)
+    for copy in small:
+        copy.start()
+    for h in range(heads):
+        for a in range(2):
+            own_in(a, h).start()
     pl.semaphore_wait(barrier, n + m - 2)
-
-    def lanes_of(device, h):
-        return pl.ds(pl.multiple_of(device * cols + h * LANES, LANES), LANES)
-
-    def tokens_of(device):
-        return pl.ds(pl.multiple_of(device * tok, tok), tok)
 
     def part_of(device):
         return pl.ds(pl.multiple_of(device * q, q), q)
@@ -327,11 +334,6 @@
             device_id_type=pl.DeviceIdType.MESH,
         )
 
-    def own_in(a, h):
-        return pltpu.make_async_copy(
-            inputs[a].at[0, :, lanes_of(me, h)], s["xin"].at[a, h, tokens_of(me), :], s["own_in"].at[a, h]
-        )
-
     def own_out(h):
         return pltpu.make_async_copy(
             s["gout"].at[h, tokens_of(me), :], out_ref.at[0, :, lanes_of(me, h)], s["own_out"].at[h]
@@ -383,9 +385,6 @@
     for h in range(heads):
         for a in range(2):
             each(n, lambda o: in_copy(a, h, o).start())
-    for h in range(heads):
-        for a in range(2):
-            own_in(a, h).start()
     for copy in small:
         copy.wait()
 
@@ -437,6 +436,11 @@
             s["spike"][h, b : b + 1, :] = spike_ref[0, h : h + 1, b * LANES : (b + 1) * LANES]
     lax.fori_loop(0, heads, one_head, 0)
     each(m, lambda o: tap_copy(o).start())
+    for h in range(heads):
+        for a in range(2):
+            each(n, lambda o: in_copy(a, h, o).wait_send())
+    for h in range(heads - 1):
+        each(m, lambda o: rs_copy(h, o).wait_send())
     finish_rs(heads - 1)
     each(m, lambda o: tap_copy(o).wait_recv())
 
@@ -449,18 +453,17 @@
     for h in range(heads):
         each(m, lambda o: ag_copy(h, o).wait_recv())
         maps_out(h).start()
-    for h in range(heads):
-        each(n, lambda o: out_copy(h, o).wait_recv())
-    for h in range(heads):
-        for a in range(2):
-            each(n, lambda o: in_copy(a, h, o).wait_send())
-        each(n, lambda o: out_copy(h, o).wait_send())
-        each(m, lambda o: rs_copy(h, o).wait_send())
+    each(m, lambda o: rs_copy(heads - 1, o).wait_send())
+    for h in range(heads):
         each(m, lambda o: ag_copy(h, o).wait_send())
         own_out(h).wait()
-        maps_out(h).wait()
     each(m, lambda o: tap_copy(o).wait_send())
     tap_out.wait()
+    for h in range(heads):
+        each(n, lambda o: out_copy(h, o).wait_recv())
+    for h in range(heads):
+        each(n, lambda o: out_copy(h, o).wait_send())
+        maps_out(h).wait()
 
 
 def finish_kernel(heads, in_ref, maps_ref, tap_ref, out_ref, grate_ref, ginput_ref, gtaps_ref,

time: 49.8 us -> 49.7 us (level)
  no operation moved by 1% of the time
where the time goes in v3:
time: 49.7 us; the launch traced here: 49.5 us
  Pallas kernels  48.9 us (98%)
  between operations  0.64 us (1%)
    pallas_call x1, Pallas kernels, body(): pl.pallas_call(functools.partial(whole_kernel, (n, m, heads, tok, rows, q...  46.5 us
    pallas_call x1, Pallas kernels, body(): pl.pallas_call(functools.partial(finish_kernel, heads), in_specs=[anywher...  2.4 us

profile of v3, /device:TPU:0, one launch (start us, length us, event | category | flops | bytes accessed | tf_op | source)
XLA Modules:
  0.0 49.5 jit_solution(15845799714074687793)
XLA Ops:
  0.6 46.5 %heads_and_exchange.1 = (bf16[1,128,2048]{2,1,0:T(8,128)(2,1)}, bf16[4,512,128]{2,1,0:T(8,128)(2,1)}, f32[4,8,128]{2,1,0:T(8,128)}) custom-call(bf16[1,128,2048]{2,1,0:T(8,128)(2,1)} %x_ref.1, bf16[1,128,2048]{2,1,0:T(8,128)(2,1)} %c_ref.1, bf16[4,512]{1,0:T(4,128)(2,1)} %taps_hbm.1, bf16[2,4,128,128]{3,2,1,0:T(8,128)(2,1)} %rmap_hbm.1, ...), custom_call_target="tpu_custom_call" | custom-call | tf_op jit(solution)/shard_map/heads_and_exchange/pallas_call | solution.py:544
  47.1 2.4 %finish.1 = (bf16[1,128,2048]{2,1,0:T(8,128)(2,1)}, f32[2,4,128,128]{3,2,1,0:T(8,128)}, f32[2,4,128,128]{3,2,1,0:T(8,128)}, f32[4,512]{1,0:T(4,128)}) custom-call(bf16[1,128,2048]{2,1,0:T(8,128)(2,1)} %get-tuple-element.7.in_ref, bf16[4,512,128]{2,1,0:T(8,128)(2,1)} %get-tuple-element.8.maps_ref, f32[4,8,128]{2,1,0:T(8,128)} %get-tuple-element.9.tap_ref), custom_call_target="tpu_custom_call" | custom-call | tf_op jit(solution)/shard_map/finish/pallas_call | solution.py:567
